TPU v7x, 32 devices: a whole 2x2x4 slice. The times are simulated.
32 devices in a mesh: rep: 2 (over x), fs: 8 (over z, y), tp: 2 (over core).
Axes of the slice: x: 2, y: 2, z: 4, core: 2. Of those that a mesh axis runs over, the one named last changes fastest.
Arguments:
- tokens: bfloat16 [4096, 2048], P(('rep', 'fs', 'tp')), may hold values from -6 to 6
- mix_gain: float32 [2048], replicated, may hold values from 0.1 to 1.9
- conv_in_weight: bfloat16 [2048, 1024], P('fs', 'tp'), may hold values from -0.125 to 0.125
- gate_outer_weight: bfloat16 [2048, 1024], P('fs', 'tp'), may hold values from -0.125 to 0.125
- gate_inner_weight: bfloat16 [2048, 1024], P('fs', 'tp'), may hold values from -0.125 to 0.125
- conv_taps: float32 [3, 1024], P(None, 'tp'), may hold values from -3.5 to 3.5
- out_weight: bfloat16 [1024, 2048], P('tp', 'fs'), may hold values from -0.1875 to 0.1875
- ff_gain: float32 [2048], replicated, may hold values from 0.1 to 1.9
- up_weight: bfloat16 [2048, 8192], P('fs', 'tp'), may hold values from -0.125 to 0.125
- down_weight: bfloat16 [8192, 2048], P('tp', 'fs'), may hold values from -0.0625 to 0.0625
Outputs:
- layer_out: bfloat16 [4096, 2048], P(('rep', 'fs', 'tp'))
All inputs are finite; a program needn't handle non-finite values.
Results may differ from a plain program's by a relative error of at most 0.023.
Values may be sent and summed in bfloat16 or wider, within the bound.
A program may use at most 128 MiB of HBM per device.

v0:
```python
import jax
import jax.numpy as jnp
from jax import lax
from jax.sharding import PartitionSpec as P

eps = 1e-06


def rms_scale(values, gain):
    widened = values.astype(jnp.float32)
    inverse = lax.rsqrt(jnp.mean(widened * widened, axis=-1, keepdims=True) + eps)
    return (widened * inverse * gain).astype(jnp.bfloat16)


def on_device(
    tokens,
    mix_gain,
    conv_in_weight,
    gate_outer_weight,
    gate_inner_weight,
    conv_taps,
    out_weight,
    ff_gain,
    up_weight,
    down_weight,
):
    normed = rms_scale(tokens, mix_gain)
    gathered = lax.all_gather(normed, "tp", axis=0, tiled=True)
    seq_rows = gathered.shape[0]
    segment = (
        lax.all_gather(conv_in_weight, "fs", axis=0, tiled=True),
        lax.all_gather(gate_outer_weight, "fs", axis=0, tiled=True),
        lax.all_gather(gate_inner_weight, "fs", axis=0, tiled=True),
    )
    conv_input, gate_outer, gate_inner = tuple(
        (jnp.dot(gathered, weight, preferred_element_type=jnp.float32) for weight in segment)
    )
    conv_input = conv_input.astype(jnp.bfloat16)
    gate_outer = gate_outer.astype(jnp.bfloat16)
    gate_inner = gate_inner.astype(jnp.bfloat16)
    gated = gate_inner.astype(jnp.float32) * conv_input.astype(jnp.float32)
    padded = jnp.pad(gated, ((2, 0), (0, 0)))
    convolved = (
        conv_taps[0] * padded[0:seq_rows]
        + conv_taps[1] * padded[1 : seq_rows + 1]
        + conv_taps[2] * padded[2 : seq_rows + 2]
    )
    mixed = (gate_outer.astype(jnp.float32) * convolved).astype(jnp.bfloat16)
    out_full = lax.all_gather(out_weight, "fs", axis=1, tiled=True)
    lefts = mixed
    mix_total = lax.psum_scatter(
        jnp.dot(lefts, out_full, preferred_element_type=jnp.float32).astype(jnp.bfloat16),
        "tp",
        scatter_dimension=0,
        tiled=True,
    ).astype(jnp.float32)
    resid = (tokens.astype(jnp.float32) + mix_total).astype(jnp.bfloat16)
    normed_ff = rms_scale(resid, ff_gain)
    ff_gathered = lax.all_gather(normed_ff, "tp", axis=0, tiled=True)
    up_full = lax.all_gather(up_weight, "fs", axis=0, tiled=True)
    preact = jnp.dot(ff_gathered, up_full, preferred_element_type=jnp.float32)
    hidden = jnp.square(jax.nn.relu(preact)).astype(jnp.bfloat16)
    down_full = lax.all_gather(down_weight, "fs", axis=1, tiled=True)
    lefts = hidden
    ff_total = lax.psum_scatter(
        jnp.dot(lefts, down_full, preferred_element_type=jnp.float32).astype(jnp.bfloat16),
        "tp",
        scatter_dimension=0,
        tiled=True,
    ).astype(jnp.float32)
    return (resid.astype(jnp.float32) + ff_total).astype(jnp.bfloat16)


def solution(mesh):
    in_specs = (
        P(("rep", "fs", "tp"), None),
        P(),
        P("fs", "tp"),
        P("fs", "tp"),
        P("fs", "tp"),
        P(None, "tp"),
        P("tp", "fs"),
        P(),
        P("fs", "tp"),
        P("tp", "fs"),
    )
    out_specs = P(("rep", "fs", "tp"), None)
    return jax.shard_map(
        on_device, mesh=mesh, in_specs=in_specs, out_specs=out_specs, check_vma=False
    )
```

profile of v0, /device:TPU:0, one launch (start us, length us, event | category | flops | bytes accessed | tf_op | source)
XLA Modules:
  0.0 740.0 jit_solution(13610082769893983982)
XLA Ops:
  6.5 1.2 fusion.8
  7.8 2.0 fusion.10
  9.9 0.7 all-gather.15.cloned.1.call-update
  10.6 0.7 all-gather.13.cloned.1.call-update
  12.0 0.5 all-gather.17.cloned.1.call-update
  12.6 9.2 %all-gather.9.cloned.1.call-done = bf16[256,2048]{1,0:T(8,128)(2,1)} async-done(((bf16[128,2048]{1,0:T(8,128)(2,1)}), bf16[256,2048]{1,0:T(8,128)(2,1)}) %all-gather.9.cloned.1.call-update) | async-done | bytes 1048592 | tf_op jit(solution)/shard_map/all_gather | solution.py:28
  21.7 52.4 %all-gather.15.cloned.1.call-done = bf16[2048,512]{1,0:T(8,128)(2,1)} async-done(((bf16[256,512]{1,0:T(8,128)(2,1)}), bf16[2048,512]{1,0:T(8,128)(2,1)}) %all-gather.15.cloned.1.call-update) | async-done | bytes 2097168 | tf_op jit(solution)/shard_map/all_gather | solution.py:31
  74.2 2.6 fusion.7
  76.8 47.2 %all-gather.13.cloned.1.call-done = bf16[2048,512]{1,0:T(8,128)(2,1)} async-done(((bf16[256,512]{1,0:T(8,128)(2,1)}), bf16[2048,512]{1,0:T(8,128)(2,1)}) %all-gather.13.cloned.1.call-update) | async-done | bytes 2097168 | tf_op jit(solution)/shard_map/all_gather | solution.py:33
  124.0 2.3 fusion.6
  126.3 47.3 %all-gather.11.cloned.1.call-done = bf16[2048,512]{1,0:T(8,128)(2,1)} async-done(((bf16[256,512]{1,0:T(8,128)(2,1)}), bf16[2048,512]{1,0:T(8,128)(2,1)}) %all-gather.11.cloned.1.call-update) | async-done | bytes 2097168 | tf_op jit(solution)/shard_map/all_gather | solution.py:32
  173.6 50.8 %all-gather.17.cloned.1.call-done = bf16[512,2048]{1,0:T(8,128)(2,1)} async-done(((bf16[512,256]{1,0:T(8,128)(2,1)}), bf16[512,2048]{1,0:T(8,128)(2,1)}) %all-gather.17.cloned.1.call-update) | async-done | bytes 2097168 | tf_op jit(solution)/shard_map/all_gather | solution.py:49
  224.4 4.7 convolution_convert_fusion.1
  229.2 6.7 reduce-scatter.3.cloned.1.call-done
  235.9 1.3 fusion.12
  237.2 2.0 fusion.14
  239.3 0.7 all-gather.21.cloned.1.call-update
  240.0 0.7 all-gather.23.cloned.1.call-update
  240.8 8.9 %all-gather.19.cloned.1.call-done = bf16[256,2048]{1,0:T(8,128)(2,1)} async-done(((bf16[128,2048]{1,0:T(8,128)(2,1)}), bf16[256,2048]{1,0:T(8,128)(2,1)}) %all-gather.19.cloned.1.call-update) | async-done | bytes 1048592 | tf_op jit(solution)/shard_map/all_gather | solution.py:59
  249.6 230.6 %all-gather.21.cloned.1.call-done = bf16[2048,4096]{1,0:T(8,128)(2,1)} async-done(((bf16[256,4096]{1,0:T(8,128)(2,1)}), bf16[2048,4096]{1,0:T(8,128)(2,1)}) %all-gather.21.cloned.1.call-update) | async-done | bytes 16777232 | tf_op jit(solution)/shard_map/all_gather | solution.py:60
  480.2 227.6 %all-gather.23.cloned.1.call-done = bf16[4096,2048]{1,0:T(8,128)(2,1)} async-done(((bf16[4096,256]{1,0:T(8,128)(2,1)}), bf16[4096,2048]{1,0:T(8,128)(2,1)}) %all-gather.23.cloned.1.call-update) | async-done | bytes 16777232 | tf_op jit(solution)/shard_map/all_gather | solution.py:63
  707.8 16.5 %convolution_convert_fusion = bf16[256,2048]{1,0:T(8,128)(2,1)} fusion(bf16[4096,2048]{1,0:T(8,128)(2,1)} %all-gather.23.cloned.1.call-done, bf16[256,2048]{1,0:T(8,128)(2,1)} %all-gather.19.cloned.1.call-done, bf16[2048,4096]{1,0:T(8,128)(2,1)} %all-gather.21.cloned.1.call-done), kind=kOutput, calls=%fused_computation.3 | convolution fusion | flops 8593604608 | bytes 35651584 | tf_op jit(solution)/shard_map/dot_general | solution.py:66
  724.4 6.7 reduce-scatter.5.cloned.1.call-done
  731.1 2.1 fusion.15
  (28 shorter events, 1.0 us)
Async XLA Ops:
  6.5 6.0 copy-start.4
  6.5 15.2 %all-gather.9.cloned.1.call-start = ((), (), s32[]{:S(2)}) async-start(), calls=%async_computation.2 | async-start | bytes 1572864 | tf_op jit(solution)/shard_map/all_gather | solution.py:28
  9.8 64.3 %all-gather.15.cloned.1.call-start = ((), (), s32[]{:S(2)}) async-start(), calls=%async_computation.5 | async-start | bytes 2359296 | tf_op jit(solution)/shard_map/all_gather | solution.py:31
  10.6 113.4 %all-gather.13.cloned.1.call-start = ((), (), s32[]{:S(2)}) async-start(), calls=%async_computation.4 | async-start | bytes 2359296 | tf_op jit(solution)/shard_map/all_gather | solution.py:33
  11.3 162.3 %all-gather.11.cloned.1.call-start = ((), (), s32[]{:S(2)}) async-start(), calls=%async_computation.3 | async-start | bytes 2359296 | tf_op jit(solution)/shard_map/all_gather | solution.py:32
  11.9 212.5 %all-gather.17.cloned.1.call-start = ((), (), s32[]{:S(2)}) async-start(), calls=%async_computation.6 | async-start | bytes 2359296 | tf_op jit(solution)/shard_map/all_gather | solution.py:49
  12.5 223.4 %reduce-scatter.3.cloned.1.call-start = ((), (), s32[]{:S(2)}) async-start(), calls=%async_computation.7 | async-start | bytes 1572864 | tf_op jit(solution)/shard_map/reduce_scatter | solution.py:51
  21.7 102.2 %copy-start.2 = (bf16[256,2048]{1,0:T(8,128)(2,1)S(1)}, bf16[256,2048]{1,0:T(8,128)(2,1)}, u32[]{:S(2)}) copy-start(bf16[256,2048]{1,0:T(8,128)(2,1)} %all-gather.9.cloned.1.call-done) | copy-start | bytes 3145732
  224.4 11.5 %copy-start = (bf16[128,2048]{1,0:T(8,128)(2,1)S(1)}, bf16[128,2048]{1,0:T(8,128)(2,1)}, u32[]{:S(2)}) copy-start(bf16[128,2048]{1,0:T(8,128)(2,1)} %param.10) | copy-start | bytes 1572868
  229.1 8.1 %copy-start.3 = (f32[2048]{0:T(1024)S(1)}, f32[2048]{0:T(1024)}, u32[]{:S(2)}) copy-start(f32[2048]{0:T(1024)} %param.17) | copy-start | bytes 24580
  229.1 20.5 %all-gather.19.cloned.1.call-start = ((), (), s32[]{:S(2)}) async-start(), calls=%async_computation.8 | async-start | bytes 1572864 | tf_op jit(solution)/shard_map/all_gather | solution.py:59
  239.2 241.0 %all-gather.21.cloned.1.call-start = ((), (), s32[]{:S(2)}) async-start(), calls=%async_computation.9 | async-start | bytes 18874368 | tf_op jit(solution)/shard_map/all_gather | solution.py:60
  240.0 467.8 %all-gather.23.cloned.1.call-start = ((), (), s32[]{:S(2)}) async-start(), calls=%async_computation.10 | async-start | bytes 18874368 | tf_op jit(solution)/shard_map/all_gather | solution.py:63
  240.7 490.4 %copy-start.1 = (bf16[128,2048]{1,0:T(8,128)(2,1)S(1)}, bf16[128,2048]{1,0:T(8,128)(2,1)}, u32[]{:S(2)}) copy-start(bf16[128,2048]{1,0:T(8,128)(2,1)} %reduce-scatter.3.cloned.1.call-done) | copy-start | bytes 1572868
  240.7 490.4 %reduce-scatter.5.cloned.1.call-start = ((), (), s32[]{:S(2)}) async-start(), calls=%async_computation.11 | async-start | bytes 1572864 | tf_op jit(solution)/shard_map/reduce_scatter | solution.py:65
Sparse Core Ops, SparseCore 0:
  10.0 11.7 all-gather.8
  23.9 50.2 all-gather.14
  76.3 47.6 all-gather.12
  125.9 47.6 all-gather.10
  175.5 48.8 all-gather.16
  229.2 6.5 reduce-scatter.2
  239.3 10.2 all-gather.18
  251.7 228.4 all-gather.20
  482.3 225.4 all-gather.22
  724.5 6.5 reduce-scatter.4
where the time goes:
time: 740 us
  waiting for transfers between devices  691 us (93%)
  matrix products  26.2 us (4%)
  between operations  13.6 us (2%)
  other arithmetic  8.69 us (1%)
    all_gather x1, waiting for transfers between devices, on_device(): up_full = lax.all_gather(up_weight, 'fs', axis=0, tiled=True)  231 us
    all_gather x1, waiting for transfers between devices, on_device(): down_full = lax.all_gather(down_weight, 'fs', axis=1, tiled=True)  228 us
    all_gather x1, waiting for transfers between devices, on_device(): lax.all_gather(conv_in_weight, 'fs', axis=0, tiled=True)  52.4 us
    all_gather x1, waiting for transfers between devices, on_device(): out_full = lax.all_gather(out_weight, 'fs', axis=1, tiled=True)  50.8 us
    all_gather x1, waiting for transfers between devices, on_device(): lax.all_gather(gate_outer_weight, 'fs', axis=0, tiled=True)  47.3 us
    all_gather x1, waiting for transfers between devices, on_device(): lax.all_gather(gate_inner_weight, 'fs', axis=0, tiled=True)  47.2 us
    dot_general x1, matrix products, on_device(): jnp.dot(lefts, down_full, preferred_element_type=jnp.float32)  16.5 us
  transfers between devices with their start and end apart: 10, of which 10 were waited for; matrix products, arithmetic and copies ran while one was open for 1% of the time, Pallas kernels for 0%

commit v1 on v0

v1 whole, which is shorter than its diff:
```python
import jax
import jax.numpy as jnp
from jax import lax
from jax.sharding import Mesh, PartitionSpec as P

eps = 1e-06


def rms_scale(values, gain):
    widened = values.astype(jnp.float32)
    inverse = lax.rsqrt(jnp.mean(widened * widened, axis=-1, keepdims=True) + eps)
    return (widened * inverse * gain).astype(jnp.bfloat16)


GROUP = ("rep", "near", "tp")


def gather_rows(block, near):
    rows, width = block.shape[0], block.shape[1] // near
    if near > 1:
        block = lax.all_to_all(
            block.reshape(rows, near, width).transpose(1, 0, 2), "near", 0, 0, tiled=True
        ).reshape(near * rows, width)
    return lax.all_gather(block, "far", axis=0, tiled=True)


def own_part(block, axis, rep):
    size = block.shape[axis] // rep
    return lax.dynamic_slice_in_dim(block, lax.axis_index("rep") * size, size, axis)


def on_device(rep, near, tp, tokens, mix_gain, conv_in, outer, inner, taps, out_w, ff_gain, up_w, down_w):
    seq_rows = tokens.shape[0] * tp
    depth = up_w.shape[0]
    parts = [own_part(w, 1, rep) for w in (conv_in, outer, inner)]
    width = parts[0].shape[1] // near
    trio = jnp.concatenate([p.reshape(depth, near, width) for p in parts], 2).reshape(depth, -1)
    trio = gather_rows(trio, near)
    out_part = own_part(out_w, 0, rep)
    out_part = out_part.reshape(near, width, -1).transpose(1, 0, 2).reshape(width, -1)
    out_full = gather_rows(out_part, near).reshape(-1, width, out_w.shape[1])
    up_full = gather_rows(own_part(up_w, 1, rep), near)
    down_part = own_part(down_w, 0, rep)
    hid = down_part.shape[0] // near
    down_part = down_part.reshape(near, hid, -1).transpose(1, 0, 2).reshape(hid, -1)
    down_full = gather_rows(down_part, near).reshape(-1, hid, down_w.shape[1])

    taps = own_part(taps, 1, rep)
    taps = lax.dynamic_slice_in_dim(taps, lax.axis_index("near") * width, width, 1)

    normed = lax.all_gather(rms_scale(tokens, mix_gain), GROUP, axis=0, tiled=True)
    proj = jnp.dot(normed, trio, preferred_element_type=jnp.float32).astype(jnp.bfloat16)
    proj = proj.astype(jnp.float32).reshape(-1, seq_rows, 3 * width)
    gated = proj[..., 2 * width :] * proj[..., :width]
    padded = jnp.pad(gated, ((0, 0), (2, 0), (0, 0)))
    convolved = sum(taps[k] * padded[:, k : seq_rows + k] for k in range(3))
    mixed = (proj[..., width : 2 * width] * convolved).astype(jnp.bfloat16)
    mixed = mixed.reshape(-1, width)

    def project(lefts, rights):
        whole = rights.transpose(1, 0, 2).reshape(lefts.shape[1], -1)
        partial = jnp.dot(lefts, whole, preferred_element_type=jnp.float32)
        return lax.psum_scatter(
            partial.astype(jnp.bfloat16), GROUP, scatter_dimension=0, tiled=True
        ).astype(jnp.float32)

    resid = (tokens.astype(jnp.float32) + project(mixed, out_full)).astype(jnp.bfloat16)
    normed_ff = lax.all_gather(rms_scale(resid, ff_gain), GROUP, axis=0, tiled=True)
    preact = jnp.dot(normed_ff, up_full, preferred_element_type=jnp.float32)
    hidden = jnp.square(jax.nn.relu(preact)).astype(jnp.bfloat16)
    return (resid.astype(jnp.float32) + project(hidden, down_full)).astype(jnp.bfloat16)


def solution(mesh):
    rep, fs, tp = (mesh.shape[name] for name in ("rep", "fs", "tp"))
    near = 2 if fs % 2 == 0 else 1
    mesh4 = Mesh(mesh.devices.reshape(rep, fs // near, near, tp), ("rep", "far", "near", "tp"))
    fs_axes = ("far", "near")
    rows = P(("rep", "far", "near", "tp"), None)
    in_specs = (
        rows,
        P(),
        P(fs_axes, "tp"),
        P(fs_axes, "tp"),
        P(fs_axes, "tp"),
        P(None, "tp"),
        P("tp", fs_axes),
        P(),
        P(fs_axes, "tp"),
        P("tp", fs_axes),
    )

    def body(*args):
        return on_device(rep, near, tp, *args)

    return jax.shard_map(body, mesh=mesh4, in_specs=in_specs, out_specs=rows, check_vma=False)
```

time: 740 us -> 446 us (0.60)
  waiting for transfers between devices: 691 us -> 302 us
  blocking collectives: 0 us -> 76.2 us
  local copies, waits for them, and re-layouts: 0.03 us -> 19.5 us
    all_gather x8 -> x5, waiting for transfers between devices: 674 us -> 239 us  [the longest x3 164 us: gather_rows(): return lax.all_gather(block, 'far', axis=0, tiled=True)]
    all_to_all x0 -> x3, blocking collectives: none -> 52.7 us  [gather_rows(): lax.all_to_all(block.reshape(rows, near, width).transpose(1, 0, 2), 'near...]
    reduce_scatter x2, waiting for transfers between devices: 13.4 us -> 60 us  [project(): lax.psum_scatter(partial.astype(jnp.bfloat16), GROUP, scatter_dimension=0...]
    all_gather x0 -> x1, blocking collectives: none -> 23.5 us  [gather_rows(): return lax.all_gather(block, 'far', axis=0, tiled=True)]
    transpose x0 -> x2, local copies, waits for them, and re-layouts: none -> 7.77 us  [project(): whole = rights.transpose(1, 0, 2).reshape(lefts.shape[1], -1)]
    dot_general x4 -> x3, matrix products: 26.2 us -> 22.6 us  [the longest x2 17.6 us: project(): partial = jnp.dot(lefts, whole, preferred_element_type=jnp.float32)]
  transfers between devices with their start and end apart: 10 -> 8, of which waited for: 10 -> 8; matrix products, arithmetic and copies ran while one was open for 1% -> 5% of each run, Pallas kernels for 0% -> 0%
where the time goes in v1:
time: 446 us; the launch traced here: 445 us
  waiting for transfers between devices  302 us (68%)
  blocking collectives  76.2 us (17%)
  matrix products  22.6 us (5%)
  local copies, waits for them, and re-layouts  19.5 us (4%)
  between operations  13.6 us (3%)
  other arithmetic  6.98 us (2%)
    all_gather x3, waiting for transfers between devices, gather_rows(): return lax.all_gather(block, 'far', axis=0, tiled=True)  164 us
    reduce_scatter x2, waiting for transfers between devices, project(): lax.psum_scatter(partial.astype(jnp.bfloat16), GROUP, scatter_dimension=0...  60 us
    all_to_all x3, blocking collectives, gather_rows(): lax.all_to_all(block.reshape(rows, near, width).transpose(1, 0, 2), 'near...  52.7 us
    all_gather x1, waiting for transfers between devices, on_device(): lax.all_gather(rms_scale(tokens, mix_gain), GROUP, axis=0, tiled=True)  37.4 us
    all_gather x1, waiting for transfers between devices, on_device(): lax.all_gather(rms_scale(resid, ff_gain), GROUP, axis=0, tiled=True)  36.8 us
    all_gather x1, blocking collectives, gather_rows(): return lax.all_gather(block, 'far', axis=0, tiled=True)  23.5 us
    dot_general x2, matrix products, project(): partial = jnp.dot(lefts, whole, preferred_element_type=jnp.float32)  17.6 us
  transfers between devices with their start and end apart: 8, of which 8 were waited for; matrix products, arithmetic and copies ran while one was open for 5% of the time, Pallas kernels for 0%

profile of v1, /device:TPU:0, one launch (start us, length us, event | category | flops | bytes accessed | tf_op | source)
XLA Modules:
  0.0 444.9 jit_solution(15494515364846325510)
XLA Ops:
  9.0 10.6 %all_to_all.20 = bf16[2,256,384]{1,2,0:T(8,128)(2,1)S(1)} all-to-all(bf16[2,256,384]{1,2,0:T(8,128)(2,1)S(1)} %maximum_bitcast_fusion), channel_id=1, replica_groups=mesh['rep'=2,'far'=4,'near'=2,'tp'=2] {'near'}, dimensions={0} | all-to-all | bytes 786432 | tf_op jit(solution)/shard_map/all_to_all | solution.py:21
  22.6 3.4 all-to-all-start.1
  26.8 3.6 all-to-all-done.1
  30.4 23.5 %all_gather.20 = bf16[1024,256]{1,0:T(8,128)(2,1)} all-gather(bf16[256,256]{1,0:T(8,128)(2,1)S(1)} %bitcast.49), channel_id=1, replica_groups=mesh['rep'=2,'far'=4,'near'=2,'tp'=2] {'far'}, dimensions={0}, use_global_device_ids=true | all-gather | bytes 655360 | tf_op jit(solution)/shard_map/all_gather | solution.py:24
  53.9 1.3 copy.15
  55.2 11.4 %all-gather.8.cloned.1.call-done = bf16[2048,384]{1,0:T(8,128)(2,1)} async-done(((bf16[512,384]{1,0:T(8,128)(2,1)}), bf16[2048,384]{1,0:T(8,128)(2,1)}) %all-gather.8.cloned.1.call-update) | async-done | bytes 1572880 | tf_op jit(solution)/shard_map/all_gather | solution.py:24
  66.6 37.4 %all-gather.6.cloned.1.call-done = bf16[1024,2048]{1,0:T(8,128)(2,1)} async-done(((bf16[128,2048]{1,0:T(8,128)(2,1)}), bf16[1024,2048]{1,0:T(8,128)(2,1)}) %all-gather.6.cloned.1.call-update) | async-done | bytes 4194320 | tf_op jit(solution)/shard_map/all_gather | solution.py:51
  104.0 5.0 %convolution_convert_fusion.2 = bf16[1024,384]{1,0:T(8,128)(2,1)S(1)} fusion(bf16[1024,2048]{1,0:T(8,128)(2,1)} %all-gather.6.cloned.1.call-done, bf16[2048,384]{1,0:T(8,128)(2,1)} %all-gather.8.cloned.1.call-done), kind=kOutput, calls=%fused_computation.9 | convolution fusion | flops 1611005952 | bytes 6553600 | tf_op jit(solution)/shard_map/dot_general | solution.py:52
  109.3 3.2 convolution_convert_fusion
  112.7 17.6 %all_to_all.21 = bf16[2,1024,256]{2,1,0:T(8,128)(2,1)} all-to-all(bf16[2,1024,256]{2,1,0:T(8,128)(2,1)S(1)} %bitcast.38), channel_id=1, replica_groups=mesh['rep'=2,'far'=4,'near'=2,'tp'=2] {'near'}, dimensions={0} | all-to-all | bytes 2097152 | tf_op jit(solution)/shard_map/all_to_all | solution.py:21
  130.4 2.3 constant_dynamic-slice_fusion.1
  132.7 2.3 copy.22
  135.0 24.5 %all_to_all.22 = bf16[2,256,1024]{1,2,0:T(8,128)(2,1)} all-to-all(bf16[2,256,1024]{1,2,0:T(8,128)(2,1)} %bitcast.43), channel_id=1, replica_groups=mesh['rep'=2,'far'=4,'near'=2,'tp'=2] {'near'}, dimensions={0} | all-to-all | bytes 2097152 | tf_op jit(solution)/shard_map/all_to_all | solution.py:21
  159.5 2.3 copy.17
  161.9 8.7 %reduce-scatter.3.cloned.1.call-done = bf16[128,2048]{1,0:T(8,128)(2,1)} async-done(((bf16[1024,2048]{1,0:T(8,128)(2,1)}), bf16[128,2048]{1,0:T(8,128)(2,1)}) %reduce-scatter.3.cloned.1.call-update) | async-done | bytes 524304 | tf_op jit(solution)/shard_map/reduce_scatter | solution.py:63
  170.6 1.3 fusion.4
  171.9 2.0 fusion.6
  174.0 78.8 %all-gather.14.cloned.1.call-done = bf16[8192,256]{1,0:T(8,128)(2,1)} async-done(((bf16[2048,256]{1,0:T(8,128)(2,1)}), bf16[8192,256]{1,0:T(8,128)(2,1)}) %all-gather.14.cloned.1.call-update) | async-done | bytes 4194320 | tf_op jit(solution)/shard_map/all_gather | solution.py:24
  252.8 6.5 %copy.18 = bf16[1024,8,256]{0,2,1:T(8,128)(2,1)} copy(bf16[1024,8,256]{2,0,1:T(8,128)(2,1)} %bitcast.39) | data formatting | bytes 8388608 | tf_op jit(solution)/shard_map/transpose | solution.py:61
  259.3 74.2 %all-gather.12.cloned.1.call-done = bf16[2048,1024]{1,0:T(8,128)(2,1)} async-done(((bf16[512,1024]{1,0:T(8,128)(2,1)}), bf16[2048,1024]{1,0:T(8,128)(2,1)}) %all-gather.12.cloned.1.call-update) | async-done | bytes 4194320 | tf_op jit(solution)/shard_map/all_gather | solution.py:24
  333.5 36.8 %all-gather.10.cloned.1.call-done = bf16[1024,2048]{1,0:T(8,128)(2,1)} async-done(((bf16[128,2048]{1,0:T(8,128)(2,1)}), bf16[1024,2048]{1,0:T(8,128)(2,1)}) %all-gather.10.cloned.1.call-update) | async-done | bytes 4194320 | tf_op jit(solution)/shard_map/all_gather | solution.py:68
  370.3 14.4 %convolution_convert_fusion.1 = bf16[1024,2048]{1,0:T(8,128)(2,1)} fusion(bf16[1024,2048]{0,1:T(8,128)(2,1)} %bitcast.40, bf16[1024,2048]{1,0:T(8,128)(2,1)} %all-gather.10.cloned.1.call-done, bf16[2048,1024]{1,0:T(8,128)(2,1)} %all-gather.12.cloned.1.call-done), kind=kOutput, calls=%fused_computation.2 | convolution fusion | flops 8595177472 | bytes 16777216 | tf_op jit(solution)/shard_map/dot_general | solution.py:62
  384.7 51.3 %reduce-scatter.5.cloned.1.call-done = bf16[128,2048]{1,0:T(8,128)(2,1)} async-done(((bf16[1024,2048]{1,0:T(8,128)(2,1)}), bf16[128,2048]{1,0:T(8,128)(2,1)}) %reduce-scatter.5.cloned.1.call-update) | async-done | bytes 524304 | tf_op jit(solution)/shard_map/reduce_scatter | solution.py:63
  436.0 2.1 fusion.7
  (44 shorter events, 6.8 us)
Async XLA Ops:
  6.5 106.1 %copy-start = (bf16[4096,256]{1,0:T(8,128)(2,1)S(1)}, bf16[4096,256]{1,0:T(8,128)(2,1)}, u32[]{:S(2)}) copy-start(bf16[4096,256]{1,0:T(8,128)(2,1)} %param.19) | copy-start | bytes 6291460
  6.5 14.1 %copy-start.1 = (bf16[128,2048]{1,0:T(8,128)(2,1)S(1)}, bf16[128,2048]{1,0:T(8,128)(2,1)}, u32[]{:S(2)}) copy-start(bf16[128,2048]{1,0:T(8,128)(2,1)} %param.10) | copy-start | bytes 1572868
  6.5 14.3 %copy-start.4 = (f32[2048]{0:T(1024)S(1)}, f32[2048]{0:T(1024)}, u32[]{:S(2)}) copy-start(f32[2048]{0:T(1024)} %param.11) | copy-start | bytes 24580
  6.5 15.3 %copy-start.3 = (bf16[512,256]{1,0:T(8,128)(2,1)S(1)}, bf16[512,256]{1,0:T(8,128)(2,1)}, u32[]{:S(2)}) copy-start(bf16[512,256]{1,0:T(8,128)(2,1)} %param.16) | copy-start | bytes 786436
  6.5 60.1 %all-gather.8.cloned.1.call-start = ((), (), s32[]{:S(2)}) async-start(), calls=%async_computation.7 | async-start | bytes 1966080 | tf_op jit(solution)/shard_map/all_gather | solution.py:24
  20.6 83.4 %all-gather.6.cloned.1.call-start = ((), (), s32[]{:S(2)}) async-start(), calls=%async_computation.6 | async-start | bytes 4718592 | tf_op jit(solution)/shard_map/all_gather | solution.py:51
  22.6 7.8 %all-to-all-start.1 = ((bf16[2,128,256]{2,1,0:T(8,128)(2,1)}), bf16[2,128,256]{2,1,0:T(8,128)(2,1)S(1)}, u32[]{:S(2)}, u32[]{:S(2)}) async-start(bf16[2,128,256]{2,1,0:T(8,128)(2,1)} %bitcast.11), calls=%async_computation.1 | async-start | bytes 262144 | tf_op jit(solution)/shard_map/all_to_all | solution.py:21
  25.9 144.7 %reduce-scatter.3.cloned.1.call-start = ((), (), s32[]{:S(2)}) async-start(), calls=%async_computation.8 | async-start | bytes 4718592 | tf_op jit(solution)/shard_map/reduce_scatter | solution.py:63
  112.6 140.2 %all-gather.14.cloned.1.call-start = ((), (), s32[]{:S(2)}) async-start(), calls=%async_computation.11 | async-start | bytes 5242880 | tf_op jit(solution)/shard_map/all_gather | solution.py:24
  130.3 203.2 %all-gather.12.cloned.1.call-start = ((), (), s32[]{:S(2)}) async-start(), calls=%async_computation.10 | async-start | bytes 5242880 | tf_op jit(solution)/shard_map/all_gather | solution.py:24
  132.7 39.2 %copy-start.5 = (f32[2048]{0:T(1024)S(1)}, f32[2048]{0:T(1024)}, u32[]{:S(2)}) copy-start(f32[2048]{0:T(1024)} %param.17) | copy-start | bytes 24580
  161.8 208.5 %all-gather.10.cloned.1.call-start = ((), (), s32[]{:S(2)}) async-start(), calls=%async_computation.9 | async-start | bytes 4718592 | tf_op jit(solution)/shard_map/all_gather | solution.py:68
  174.0 262.0 %reduce-scatter.5.cloned.1.call-start = ((), (), s32[]{:S(2)}) async-start(), calls=%async_computation.12 | async-start | bytes 4718592 | tf_op jit(solution)/shard_map/reduce_scatter | solution.py:63
  384.7 51.3 %copy-start.2 = (bf16[128,2048]{1,0:T(8,128)(2,1)S(1)}, bf16[128,2048]{1,0:T(8,128)(2,1)}, u32[]{:S(2)}) copy-start(bf16[128,2048]{1,0:T(8,128)(2,1)} %reduce-scatter.3.cloned.1.call-done) | copy-start | bytes 1572868
Sparse Core Ops, SparseCore 0:
  20.7 45.8 all-gather.7
  68.5 35.4 all-gather.5
  112.7 57.8 reduce-scatter.2
  172.0 80.7 all-gather.13
  254.2 79.2 all-gather.11
  335.2 35.0 all-gather.9
  384.8 51.1 reduce-scatter.4

commit v2 on v1

--- a/solution.py
+++ b/solution.py
@@ -1,6 +1,10 @@
+import functools
+
 import jax
 import jax.numpy as jnp
 from jax import lax
+from jax.experimental import pallas as pl
+from jax.experimental.pallas import tpu as pltpu
 from jax.sharding import Mesh, PartitionSpec as P
 
 eps = 1e-06
@@ -69,6 +73,346 @@
     preact = jnp.dot(normed_ff, up_full, preferred_element_type=jnp.float32)
     hidden = jnp.square(jax.nn.relu(preact)).astype(jnp.bfloat16)
     return (resid.astype(jnp.float32) + project(hidden, down_full)).astype(jnp.bfloat16)
+
+
+def visit_order(far):
+    return [sorted(range(far), key=lambda s: (abs(s - z), s)) for z in range(far)]
+
+
+def layer_kernel(
+    far,
+    tok_ref, mix_gain_ref, conv_ref, outer_ref, inner_ref, taps_ref, outw_ref, ff_gain_ref, upw_ref, dnw_ref,
+    o_ref,
+    trio, outb, upb, dnb, stage, toks, toks_ff, part, sib, rsend, rrecv, part_ff, sib_ff, rsend_ff, rrecv_ff,
+    hidden, resid,
+    local_sem, stage_sem, near_send, right_send, left_send, w_recv,
+    ag_send, ag_recv, sib_send, sib_recv, rs_send, rs_recv,
+):
+    r, z, y, t = (lax.axis_index(name) for name in ("rep", "far", "near", "tp"))
+    m = r * 2 + y
+    rows = tok_ref.shape[0]
+    seq = 2 * rows
+    width = trio.shape[1] // 3
+    depth, hid = upw_ref.shape[0], upb.shape[1]
+    cols = dnw_ref.shape[1]
+    bf16, f32 = jnp.bfloat16, jnp.float32
+
+    def al(v, n):
+        return pl.multiple_of(v, n)
+
+    def push(a, b, s, q, where):
+        return pltpu.make_async_remote_copy(
+            src_ref=a, dst_ref=b, send_sem=s, recv_sem=q, device_id=where, device_id_type=pl.DeviceIdType.MESH
+        )
+
+    def chip(c):
+        return (lax.div(c, 2), z, lax.rem(c, 2), t)
+
+    sibling = (r, z, y, 1 - t)
+    beside = (r, z, 1 - y, t)
+
+    def place(k, zs, ys):
+        p = zs * 2 + ys
+        if k == 0:
+            return trio.at[pl.ds(al(p * depth, depth), depth), :]
+        if k == 1:
+            return outb.at[:, pl.ds(al(p * cols, cols), cols)]
+        if k == 2:
+            return upb.at[pl.ds(al(p * depth, depth), depth), :]
+        return dnb.at[:, pl.ds(al(p * cols, cols), cols)]
+
+    def share(k, ys):
+        q = r * 2 + ys
+        if k == 1:
+            return outw_ref.at[pl.ds(al(q * width, width), width), :]
+        if k == 2:
+            return upw_ref.at[:, pl.ds(al(q * hid, hid), hid)]
+        return dnw_ref.at[pl.ds(al(q * hid, hid), hid), :]
+
+    trio_in = (conv_ref, outer_ref, inner_ref)
+
+    def trio_copies(dst, ys, sems):
+        q = r * 2 + ys
+        return [
+            pltpu.make_async_copy(
+                w.at[:, pl.ds(al(q * width, width), width)],
+                dst.at[:, pl.ds(j * width, width)],
+                sems.at[j],
+            )
+            for j, w in enumerate(trio_in)
+        ]
+
+    own_trio = trio_copies(place(0, z, y), y, local_sem)
+    other_trio = trio_copies(stage, 1 - y, stage_sem)
+    own_rest = [None] + [pltpu.make_async_copy(share(k, y), place(k, z, y), local_sem.at[2 + k]) for k in (1, 2, 3)]
+    for copy in other_trio + own_trio + own_rest[1:]:
+        copy.start()
+
+    def near_copy(k):
+        a = stage if k == 0 else share(k, 1 - y)
+        return push(a, place(k, z, y), near_send.at[k], w_recv.at[k, z * 2 + y], beside)
+
+    def hop(k, zs, ys, step, sems):
+        p = zs * 2 + ys
+        at = place(k, zs, ys)
+        return push(at, at, sems.at[k, p], w_recv.at[k, p], (r, z + step, y, t))
+
+    order = visit_order(far)
+
+    def nth(j):
+        zs = jnp.int32(order[0][j])
+        for c in range(1, far):
+            zs = jnp.where(z == c, order[c][j], zs)
+        return zs
+
+    def send_on(k, zs, ys):
+        @pl.when(jnp.logical_and(zs <= z, z + 1 < far))
+        def _():
+            hop(k, zs, ys, 1, right_send).start()
+
+        @pl.when(jnp.logical_and(zs >= z, z > 0))
+        def _():
+            hop(k, zs, ys, -1, left_send).start()
+
+    def arrive_own(k):
+        for copy in own_trio if k == 0 else [own_rest[k]]:
+            copy.wait()
+        send_on(k, z, y)
+
+    def arrive_beside(k):
+        push(place(k, z, 1 - y), place(k, z, 1 - y), near_send.at[k], w_recv.at[k, z * 2 + 1 - y], beside).wait_recv()
+        send_on(k, z, 1 - y)
+
+    def arrive(k, j):
+        zs = nth(j)
+        for ys in (y, 1 - y):
+            push(
+                place(k, zs, ys), place(k, zs, ys), near_send.at[k], w_recv.at[k, zs * 2 + ys], beside
+            ).wait_recv()
+            send_on(k, zs, ys)
+        return zs
+
+    def norm(values, gain_ref):
+        inverse = lax.rsqrt(jnp.mean(values * values, axis=-1, keepdims=True) + eps)
+        return (values * inverse * gain_ref[...]).astype(bf16)
+
+    def slot(buf, c, core):
+        return buf.at[pl.ds(al((c * 2 + core) * rows, rows), rows), :]
+
+    def ag_copy(g, buf, i):
+        at = slot(buf, m, t)
+        where = sibling if i == 3 else chip(lax.rem(m + 1 + i, 4))
+        return push(at, at, ag_send.at[g, i], ag_recv.at[g, m * 2 + t], where)
+
+    def ag_relay(g, buf, i):
+        c = lax.rem(m + 3 - i, 4)
+        at = slot(buf, c, t)
+        return push(at, at, ag_send.at[g, 4 + i], ag_recv.at[g, c * 2 + t], sibling)
+
+    def ag_start(g, buf):
+        for i in range(4):
+            ag_copy(g, buf, i).start()
+
+    def ag_wait(g, buf, c, core):
+        at = slot(buf, c, core)
+        push(at, at, ag_send.at[g, 0], ag_recv.at[g, c * 2 + core], sibling).wait_recv()
+
+    def ag_finish(g, buf):
+        for i in (0, 2, 1):
+            ag_wait(g, buf, lax.rem(m + 3 - i, 4), t)
+            ag_relay(g, buf, i).start()
+        for i in range(4):
+            ag_wait(g, buf, lax.rem(m + 3 - i, 4), 1 - t)
+
+    for copy in other_trio:
+        copy.wait()
+    near_copy(0).start()
+    near_copy(1).start()
+    arrive_own(0)
+    arrive_own(1)
+    toks[pl.ds(al((m * 2 + t) * rows, rows), rows), :] = norm(tok_ref[...].astype(f32), mix_gain_ref)
+    ag_start(0, toks)
+    near_copy(2).start()
+    near_copy(3).start()
+    for k in (0, 1):
+        arrive_beside(k)
+    for j in range(1, far):
+        for k in (0, 1):
+            arrive(k, j)
+        if j == 1:
+            ag_finish(0, toks)
+    arrive_own(2)
+    arrive_beside(2)
+
+    mix_cols = outb.shape[1]
+    q = r * 2 + y
+    taps = taps_ref[:, pl.ds(al(q * width, width), width)]
+
+    def sib_copy(g, n, s, buf, land, lo, size):
+        at = buf.at[pl.ds(al(s * seq + (1 - t) * rows, rows), rows), pl.ds(lo, size)]
+        to = land.at[pl.ds(al(s * rows, rows), rows), pl.ds(lo, size)]
+        return push(at, to, sib_send.at[n, s], sib_recv.at[n, s], sibling)
+
+    def rs_copy(n, i, send, land, lo, size):
+        at = send.at[i, :, pl.ds(lo, size)]
+        return push(at, land.at[i, :, pl.ds(lo, size)], rs_send.at[n, i], rs_recv.at[n, i], chip(lax.rem(m + 1 + i, 4)))
+
+    def rs_middle(g, n, buf, land, send, rland, lo, size):
+        for i in range(4):
+            s = lax.rem(m + 1 + i, 4)
+            sib_copy(g, n, s, buf, land, lo, size).wait_recv()
+            total = (
+                buf[pl.ds(al(s * seq + t * rows, rows), rows), pl.ds(lo, size)].astype(f32)
+                + land[pl.ds(al(s * rows, rows), rows), pl.ds(lo, size)].astype(f32)
+            )
+            send[i, :, pl.ds(lo, size)] = total.astype(bf16)
+            if i < 3:
+                rs_copy(n, i, send, rland, lo, size).start()
+
+    def rs_total(n, send, rland, lo, size):
+        total = send[3, :, pl.ds(lo, size)].astype(f32)
+        for i in range(3):
+            rs_copy(n, i, send, rland, lo, size).wait_recv()
+            total = total + rland[i, :, pl.ds(lo, size)].astype(f32)
+        return total
+
+    @pl.loop(0, 4)
+    def _(i):
+        s = lax.rem(m + 1 + i, 4)
+        x = toks[pl.ds(al(s * seq, seq), seq), :]
+        proj = jnp.dot(x, trio[...], preferred_element_type=f32).astype(bf16).astype(f32)
+        gated = proj[:, 2 * width :] * proj[:, :width]
+        row = lax.broadcasted_iota(jnp.int32, gated.shape, 0)
+        back1 = jnp.where(row < 1, 0.0, pltpu.roll(gated, 1, 0))
+        back2 = jnp.where(row < 2, 0.0, pltpu.roll(gated, 2, 0))
+        convolved = taps[0:1] * back2 + taps[1:2] * back1 + taps[2:3] * gated
+        mixed = (proj[:, width : 2 * width] * convolved).astype(bf16)
+        for lo in range(0, mix_cols, 1024):
+            size = min(1024, mix_cols - lo)
+            part[pl.ds(al(s * seq, seq), seq), pl.ds(lo, size)] = jnp.dot(
+                mixed, outb[:, pl.ds(lo, size)], preferred_element_type=f32
+            ).astype(bf16)
+        sib_copy(0, 0, s, part, sib, 0, mix_cols).start()
+
+    rs_middle(0, 0, part, sib, rsend, rrecv, 0, mix_cols)
+    arrive(2, 1)
+    resid[...] = (tok_ref[...].astype(f32) + rs_total(0, rsend, rrecv, 0, mix_cols)).astype(bf16)
+    toks_ff[pl.ds(al((m * 2 + t) * rows, rows), rows), :] = norm(resid[...].astype(f32), ff_gain_ref)
+    ag_start(1, toks_ff)
+    for j in range(2, far):
+        arrive(2, j)
+        if j == 2:
+            ag_finish(1, toks_ff)
+    if far < 3:
+        ag_finish(1, toks_ff)
+    arrive_own(3)
+    arrive_beside(3)
+
+    @pl.loop(0, 4)
+    def _(s):
+        x = toks_ff[pl.ds(al(s * seq, seq), seq), :]
+        half = hid // 2
+        for lo in (0, half):
+            act = jnp.dot(x, upb[:, pl.ds(lo, half)], preferred_element_type=f32)
+            hidden[pl.ds(al(s * seq, seq), seq), pl.ds(lo, half)] = jnp.square(jnp.maximum(act, 0.0)).astype(bf16)
+
+    group = 2 * cols
+
+    def down(zs):
+        lo = al(zs * group, group)
+
+        @pl.loop(0, 4)
+        def _(i):
+            s = lax.rem(m + 1 + i, 4)
+            part_ff[pl.ds(al(s * seq, seq), seq), pl.ds(lo, group)] = jnp.dot(
+                hidden[pl.ds(al(s * seq, seq), seq), :], dnb[:, pl.ds(lo, group)], preferred_element_type=f32
+            ).astype(bf16)
+            sib_copy(1, 1 + zs, s, part_ff, sib_ff, lo, group).start()
+
+        rs_middle(1, 1 + zs, part_ff, sib_ff, rsend_ff, rrecv_ff, lo, group)
+
+    down(z)
+    for j in range(1, far):
+        down(arrive(3, j))
+    for j in range(far):
+        zs = nth(j)
+        lo = al(zs * group, group)
+        total = rs_total(1 + zs, rsend_ff, rrecv_ff, lo, group)
+        o_ref[:, pl.ds(lo, group)] = (resid[:, pl.ds(lo, group)].astype(f32) + total).astype(bf16)
+
+    for k in range(4):
+        near_copy(k).wait_send()
+        for zs in range(far):
+            for ys in range(2):
+                @pl.when(jnp.logical_and(zs <= z, z + 1 < far))
+                def _():
+                    hop(k, zs, ys, 1, right_send).wait_send()
+
+                @pl.when(jnp.logical_and(zs >= z, z > 0))
+                def _():
+                    hop(k, zs, ys, -1, left_send).wait_send()
+    for g, buf in ((0, toks), (1, toks_ff)):
+        for i in range(4):
+            ag_copy(g, buf, i).wait_send()
+        for i in range(3):
+            ag_relay(g, buf, i).wait_send()
+    for s in range(4):
+        sib_copy(0, 0, s, part, sib, 0, mix_cols).wait_send()
+        for zs in range(far):
+            sib_copy(1, 1 + zs, s, part_ff, sib_ff, zs * group, group).wait_send()
+    for i in range(3):
+        rs_copy(0, i, rsend, rrecv, 0, mix_cols).wait_send()
+        for zs in range(far):
+            rs_copy(1 + zs, i, rsend_ff, rrecv_ff, zs * group, group).wait_send()
+
+
+def fused_layer(far, tokens, mix_gain, conv_in, outer, inner, taps, out_w, ff_gain, up_w, down_w):
+    bf16 = jnp.bfloat16
+    rows, feat = tokens.shape
+    depth, cols = up_w.shape[0], down_w.shape[1]
+    width, hid = conv_in.shape[1] // 4, up_w.shape[1] // 4
+    whole = 8 * rows
+    vmem = pl.BlockSpec(memory_space=pltpu.VMEM)
+    hbm = pl.BlockSpec(memory_space=pl.ANY)
+    dma = pltpu.SemaphoreType.DMA
+    block = [
+        pltpu.VMEM((whole, feat), bf16),
+        pltpu.VMEM((4 * rows, feat), bf16),
+        pltpu.VMEM((4, rows, feat), bf16),
+        pltpu.VMEM((3, rows, feat), bf16),
+    ]
+    return pl.pallas_call(
+        functools.partial(layer_kernel, far),
+        out_shape=jax.ShapeDtypeStruct((rows, feat), bf16),
+        in_specs=[vmem, vmem, hbm, hbm, hbm, vmem, hbm, vmem, hbm, hbm],
+        out_specs=vmem,
+        scratch_shapes=[
+            pltpu.VMEM((far * 2 * depth, 3 * width), bf16),
+            pltpu.VMEM((width, far * 2 * cols), bf16),
+            pltpu.VMEM((far * 2 * depth, hid), bf16),
+            pltpu.VMEM((hid, far * 2 * cols), bf16),
+            pltpu.VMEM((depth, 3 * width), bf16),
+            pltpu.VMEM((whole, feat), bf16),
+            pltpu.VMEM((whole, feat), bf16),
+            *block,
+            *block,
+            pltpu.VMEM((whole, hid), bf16),
+            pltpu.VMEM((rows, feat), bf16),
+            dma((6,)),
+            dma((3,)),
+            dma((4,)),
+            dma((4, far * 2)),
+            dma((4, far * 2)),
+            dma((4, far * 2)),
+            dma((2, 7)),
+            dma((2, 8)),
+            dma((1 + far, 4)),
+            dma((1 + far, 4)),
+            dma((1 + far, 3)),
+            dma((1 + far, 3)),
+        ],
+        compiler_params=pltpu.CompilerParams(has_side_effects=True, vmem_limit_bytes=60 * 2**20),
+    )(tokens, mix_gain[None], conv_in, outer, inner, taps, out_w, ff_gain[None], up_w, down_w)
 
 
 def solution(mesh):
@@ -91,6 +435,8 @@
     )
 
     def body(*args):
+        if rep == 2 and near == 2 and tp == 2:
+            return fused_layer(fs // near, *args)
         return on_device(rep, near, tp, *args)
 
     return jax.shard_map(body, mesh=mesh4, in_specs=in_specs, out_specs=rows, check_vma=False)

time: 446 us -> 235 us (0.53)
  waiting for transfers between devices: 302 us -> 0 us
  Pallas kernels: 0 us -> 233 us
  blocking collectives: 76.2 us -> 0 us
  matrix products: 22.6 us -> 0 us
  local copies, waits for them, and re-layouts: 19.5 us -> 1.88 us
  between operations: 13.6 us -> 0.01 us
  other arithmetic: 6.98 us -> 0 us
    all_gather x5 -> x0, waiting for transfers between devices: 239 us -> none  [the longest x3 164 us: gather_rows(): return lax.all_gather(block, 'far', axis=0, tiled=True)]
    pallas_call x0 -> x1, Pallas kernels: none -> 233 us  [fused_layer(): pl.pallas_call(functools.partial(layer_kernel, far), out_shape=jax.ShapeD...]
    reduce_scatter x2 -> x0, waiting for transfers between devices: 60 us -> none  [project(): lax.psum_scatter(partial.astype(jnp.bfloat16), GROUP, scatter_dimension=0...]
    all_to_all x3 -> x0, blocking collectives: 52.7 us -> none  [gather_rows(): lax.all_to_all(block.reshape(rows, near, width).transpose(1, 0, 2), 'near...]
    all_gather x1 -> x0, blocking collectives: 23.5 us -> none  [gather_rows(): return lax.all_gather(block, 'far', axis=0, tiled=True)]
    dot_general x3 -> x0, matrix products: 22.6 us -> none  [the longest x2 17.6 us: project(): partial = jnp.dot(lefts, whole, preferred_element_type=jnp.float32)]
    transpose x2 -> x0, local copies, waits for them, and re-layouts: 7.77 us -> none  [project(): whole = rights.transpose(1, 0, 2).reshape(lefts.shape[1], -1)]
    dynamic_slice x6 -> x0, local copies, waits for them, and re-layouts: 5.9 us -> none  [the longest x5 5.13 us: own_part(): lax.dynamic_slice_in_dim(block, lax.axis_index('rep') * size, size, axis)]
  transfers between devices with their start and end apart: 8 -> 0, of which waited for: 8 -> 0; matrix products, arithmetic and copies ran while one was open for 5% -> 0% of each run, Pallas kernels for 0% -> 0%
where the time goes in v2:
time: 235 us
  Pallas kernels  233 us (99%)
    pallas_call x1, Pallas kernels, fused_layer(): pl.pallas_call(functools.partial(layer_kernel, far), out_shape=jax.ShapeD...  233 us

profile of v2, /device:TPU:0, one launch (start us, length us, event | category | flops | bytes accessed | tf_op | source)
XLA Modules:
  0.0 234.7 jit_solution(5633848074349343006)
XLA Ops:
  0.0 232.8 %shard_map.100 = bf16[128,2048]{1,0:T(8,128)(2,1)} custom-call(bf16[128,2048]{1,0:T(8,128)(2,1)} %tok_ref.1, f32[1,2048]{1,0:T(1,128)} %bitcast.2, bf16[256,512]{1,0:T(8,128)(2,1)} %conv_ref.1, bf16[256,512]{1,0:T(8,128)(2,1)} %outer_ref.1, bf16[256,512]{1,0:T(8,128)(2,1)} %inner_ref.1, f32[3,512]{1,0:T(4,128)} %taps_ref.1, bf16[512,256]{1,0:T(8,128)(2,1)} %outw_ref.1, ...), custom_call_target="tpu_custom_call" | custom-call | tf_op jit(solution)/shard_map/pallas_call | solution.py:384
  232.8 1.9 copy.12

commit v3 on v2

--- a/solution.py
+++ b/solution.py
@@ -236,13 +236,15 @@
     near_copy(3).start()
     for k in (0, 1):
         arrive_beside(k)
+    arrive_own(2)
+    arrive_beside(2)
     for j in range(1, far):
         for k in (0, 1):
             arrive(k, j)
         if j == 1:
             ag_finish(0, toks)
-    arrive_own(2)
-    arrive_beside(2)
+    arrive_own(3)
+    arrive_beside(3)
 
     mix_cols = outb.shape[1]
     q = r * 2 + y
@@ -305,8 +307,6 @@
             ag_finish(1, toks_ff)
     if far < 3:
         ag_finish(1, toks_ff)
-    arrive_own(3)
-    arrive_beside(3)
 
     @pl.loop(0, 4)
     def _(s):

time: 235 us -> 216 us (0.919)
  Pallas kernels: 233 us -> 214 us
    pallas_call x1, Pallas kernels: 233 us -> 214 us  [fused_layer(): pl.pallas_call(functools.partial(layer_kernel, far), out_shape=jax.ShapeD...]
where the time goes in v3:
time: 216 us
  Pallas kernels  214 us (99%)
    pallas_call x1, Pallas kernels, fused_layer(): pl.pallas_call(functools.partial(layer_kernel, far), out_shape=jax.ShapeD...  214 us

profile of v3, /device:TPU:0, one launch (start us, length us, event | category | flops | bytes accessed | tf_op | source)
XLA Modules:
  0.0 215.6 jit_solution(14396378697537829051)
XLA Ops:
  0.0 213.7 %shard_map.100 = bf16[128,2048]{1,0:T(8,128)(2,1)} custom-call(bf16[128,2048]{1,0:T(8,128)(2,1)} %tok_ref.1, f32[1,2048]{1,0:T(1,128)} %bitcast.2, bf16[256,512]{1,0:T(8,128)(2,1)} %conv_ref.1, bf16[256,512]{1,0:T(8,128)(2,1)} %outer_ref.1, bf16[256,512]{1,0:T(8,128)(2,1)} %inner_ref.1, f32[3,512]{1,0:T(4,128)} %taps_ref.1, bf16[512,256]{1,0:T(8,128)(2,1)} %outw_ref.1, ...), custom_call_target="tpu_custom_call" | custom-call | tf_op jit(solution)/shard_map/pallas_call | solution.py:384
  213.7 1.9 copy.12
